TPU v7x, 512 devices: a whole 4x4x16 slice. The times are simulated.
512 devices in a mesh: fs: 64 (over z, y), tp: 8 (over x, core).
Axes of the slice: x: 4, y: 4, z: 16, core: 2. Of those that a mesh axis runs over, the one named last changes fastest.
Arguments:
- tokens: bfloat16 [16384, 2048], P('fs'), may hold values from -6 to 6
- recurrent_input_gain: bfloat16 [2048], replicated, may hold values from 0.099609375 to 1.8984375
- recurrent_branch_weight: bfloat16 [2048, 1024], P('fs', 'tp'), may hold values from -0.125 to 0.125
- output_gate_weight: bfloat16 [2048, 1024], P('fs', 'tp'), may hold values from -0.125 to 0.125
- filter_taps: bfloat16 [4, 1024], P(None, 'tp'), may hold values from -3 to 3
- retention_gate_blocks: bfloat16 [2, 8, 128, 128], P(None, 'tp'), may hold values from -0.5 to 0.5
- input_gate_blocks: bfloat16 [2, 8, 128, 128], P(None, 'tp'), may hold values from -0.5 to 0.5
- channel_decay_rate: float32 [2, 1024], P(None, 'tp'), may hold values from 0 to 0.008, as said below
- position_log_decay: float32 [2, 16384, 1024], P(None, 'fs', 'tp'), may hold values from -0.7 to 0, as said below
- recurrent_output_weight: bfloat16 [1024, 2048], P('tp', 'fs'), may hold values from -0.1875 to 0.1875
- recurrent_output_gain: bfloat16 [2048], replicated, may hold values from 0.099609375 to 1.8984375
- feedforward_norm_gain: bfloat16 [2048], replicated, may hold values from 0.099609375 to 1.8984375
- feedforward_up_weight: bfloat16 [2048, 8192], P('fs', 'tp'), may hold values from -0.125 to 0.125
- feedforward_down_weight: bfloat16 [8192, 2048], P('tp', 'fs'), may hold values from -0.0625 to 0.0625
- feedforward_output_gain: bfloat16 [2048], replicated, may hold values from 0.099609375 to 1.8984375
Outputs:
- layer_out: bfloat16 [16384, 2048], P('fs')
Inputs may be any that keep to these rules, and one draw needn't show every extreme that they name: `channel_decay_rate`: positive rates, one for each channel and direction. `position_log_decay`: zero except at a few positions of each sequence and channel.
All inputs are finite; a program needn't handle non-finite values.
Results may differ from a plain program's by a relative error of at most 0.02.
Values may be sent and summed in bfloat16 or wider, within the bound.
No kernel may reach another device: no remote copies, remote signals or barrier semaphores. Data moves between devices by JAX's collectives and lax.ppermute only.
A program may use at most 128 MiB of HBM per device.

v0:
```python
import jax
import jax.numpy as jnp
from jax import lax
from jax.sharding import Mesh
from jax.sharding import PartitionSpec as P

FS = ("zh", "zl", "y")
Z = ("zh", "zl")
TP = ("x", "c")
EPS = 1e-06
GATE_STEEPNESS = 8.0


def spread(array, axis):
    copies = jnp.broadcast_to(array, (lax.axis_size(axis), *array.shape))
    return lax.all_to_all(copies, axis, split_axis=0, concat_axis=0, tiled=True)


def mixer_weights(array):
    width = array.shape[-1]
    pieces = spread(spread(spread(array, "zh"), "zl"), "y")
    return jnp.transpose(pieces, (2, 1, 0, 3, 4)).reshape(-1, width)


def feedforward_weights(array):
    near = spread(array, "y").reshape(-1, array.shape[-1])
    return lax.all_gather(near, Z, axis=0, tiled=True)


def summed_rows(partial):
    cores, wide = (lax.axis_size("c"), lax.axis_size("x"))
    rows, width = partial.shape
    halves = partial.astype(jnp.bfloat16).reshape(cores, rows // cores, width)
    pair = lax.all_to_all(halves, "c", split_axis=0, concat_axis=0, tiled=True)
    half = jnp.sum(pair.astype(jnp.float32), axis=0).astype(jnp.bfloat16)
    quarters = half.reshape(wide, rows // (cores * wide), width)
    several = lax.all_to_all(quarters, "x", split_axis=0, concat_axis=0, tiled=True)
    return jnp.sum(several.astype(jnp.float32), axis=0)


def all_rows(part):
    return spread(spread(part, "x"), "c").reshape(-1, part.shape[-1])


def root_norm(values, gain):
    return (
        values
        * lax.rsqrt(jnp.mean(values * values, axis=-1, keepdims=True) + EPS)
        * gain.astype(jnp.float32)
    )


def combine(earlier, later):
    return (earlier[0] * later[0], later[0] * earlier[1] + later[1])


def centred_conv(signal, taps):
    length = signal.shape[0]
    width_taps = taps.shape[0]
    left_pad = width_taps // 2
    padded = jnp.pad(signal.astype(jnp.float32), ((left_pad, width_taps - 1 - left_pad), (0, 0)))
    total = jnp.zeros(signal.shape, jnp.float32)
    for offset in range(width_taps):
        total = total + padded[offset : offset + length] * taps[offset].astype(jnp.float32)
    return total.astype(jnp.bfloat16)


def block_map(signal, matrices):
    block_width = matrices.shape[-1]
    shaped = signal.reshape(signal.shape[0], matrices.shape[0], block_width)
    mapped = jnp.einsum("tnc,ncd->tnd", shaped, matrices, preferred_element_type=jnp.float32)
    return mapped.reshape(signal.shape)


def linear_recurrence(
    convolved_output,
    retention_matrices,
    input_gate_matrices,
    decay_rate_row,
    decay_extra_block,
    reversed_scan,
):
    retention_gate = jax.nn.sigmoid(block_map(convolved_output, retention_matrices))
    admit = jax.nn.sigmoid(block_map(convolved_output, input_gate_matrices))
    logarithm_decay = -GATE_STEEPNESS * retention_gate * decay_rate_row[None, :] + decay_extra_block
    decay = jnp.exp(logarithm_decay)
    drive = jnp.sqrt(-jnp.expm1(2.0 * logarithm_decay)) * (
        admit * convolved_output.astype(jnp.float32)
    )
    _, state = lax.associative_scan(combine, (decay, drive), reverse=reversed_scan, axis=0)
    return state


def per_device(
    tokens,
    recurrent_input_gain,
    recurrent_branch_weight,
    output_gate_weight,
    filter_taps,
    retention_gate_blocks,
    input_gate_blocks,
    channel_decay_rate,
    position_log_decay,
    recurrent_output_weight,
    recurrent_output_gain,
    feedforward_norm_gain,
    feedforward_up_weight,
    feedforward_down_weight,
    feedforward_output_gain,
):
    mixer = mixer_weights(
        jnp.concatenate(
            (recurrent_branch_weight, output_gate_weight, recurrent_output_weight.T), axis=1
        )
    )
    forward = feedforward_weights(
        jnp.concatenate((feedforward_up_weight, feedforward_down_weight.T), axis=1)
    )
    channels = recurrent_branch_weight.shape[1]
    hidden_units = feedforward_up_weight.shape[1]
    normed = root_norm(tokens.astype(jnp.float32), recurrent_input_gain).astype(jnp.bfloat16)
    recur_sum = jnp.dot(normed, mixer[:, :channels], preferred_element_type=jnp.float32)
    gate_sum = jnp.dot(
        normed, mixer[:, channels : 2 * channels], preferred_element_type=jnp.float32
    )
    recur_in = recur_sum.astype(jnp.bfloat16)
    gate_in = lax.optimization_barrier(gate_sum.astype(jnp.bfloat16))
    convolved_output = lax.optimization_barrier(centred_conv(recur_in, filter_taps))
    forward_sweep = linear_recurrence(
        convolved_output,
        retention_gate_blocks[0],
        input_gate_blocks[0],
        channel_decay_rate[0],
        position_log_decay[0],
        False,
    )
    backward_sweep = linear_recurrence(
        convolved_output,
        retention_gate_blocks[1],
        input_gate_blocks[1],
        channel_decay_rate[1],
        position_log_decay[1],
        True,
    )
    hidden = ((forward_sweep + backward_sweep) * jax.nn.gelu(gate_in.astype(jnp.float32))).astype(
        jnp.bfloat16
    )
    across = (((1,), (1,)), ((), ()))
    partial_value = lax.dot_general(
        hidden, mixer[:, 2 * channels :], across, preferred_element_type=jnp.float32
    )
    mixed = summed_rows(partial_value)
    share = mixed.shape[0]
    place = lax.axis_index("c") * lax.axis_size("x") + lax.axis_index("x")
    own = lax.dynamic_slice_in_dim(tokens, place * share, share, axis=0)
    stream = lax.optimization_barrier(
        (own.astype(jnp.float32) + root_norm(mixed, recurrent_output_gain)).astype(jnp.bfloat16)
    )
    normed_ff = all_rows(
        root_norm(stream.astype(jnp.float32), feedforward_norm_gain).astype(jnp.bfloat16)
    )
    lifted_sum = jnp.dot(normed_ff, forward[:, :hidden_units], preferred_element_type=jnp.float32)
    lifted = jnp.square(jax.nn.relu(lifted_sum)).astype(jnp.bfloat16)
    lowered_part = lax.dot_general(
        lifted, forward[:, hidden_units:], across, preferred_element_type=jnp.float32
    )
    lowered = summed_rows(lowered_part)
    return all_rows(
        (stream.astype(jnp.float32) + root_norm(lowered, feedforward_output_gain)).astype(
            jnp.bfloat16
        )
    )


def solution(mesh):
    split = Mesh(mesh.devices.reshape(4, 4, 4, 4, 2), ("zh", "zl", "y", "x", "c"))
    placed = (
        P(FS, None),
        P(),
        P(FS, TP),
        P(FS, TP),
        P(None, TP),
        P(None, TP, None, None),
        P(None, TP, None, None),
        P(None, TP),
        P(None, FS, TP),
        P(TP, FS),
        P(),
        P(),
        P(FS, TP),
        P(TP, FS),
        P(),
    )
    return jax.shard_map(
        per_device, mesh=split, in_specs=placed, out_specs=P(FS, None), check_vma=False
    )
```

profile of v0, /device:TPU:1, one launch (start us, length us, event | category | flops | bytes accessed | tf_op | source)
XLA Modules:
  0.0 197.8 jit_solution(3775342261377524410)
XLA Ops:
  6.5 0.9 pad_maximum_fusion
  7.4 0.8 broadcast_in_dim.41
  8.3 5.0 %all-to-all-start.7 = ((bf16[4,32,2048]{2,1,0:T(8,128)(2,1)}), bf16[4,32,2048]{2,1,0:T(8,128)(2,1)S(1)}, u32[]{:S(2)}, u32[]{:S(2)}) async-start(bf16[4,32,2048]{2,1,0:T(8,128)(2,1)} %broadcast_in_dim.41), calls=%async_computation.7 | async-start | bytes 1048576 | tf_op jit(solution)/shard_map/all_to_all | solution.py:16
  13.3 0.7 pad_maximum_fusion.5
  14.0 6.2 %all-to-all-done.7 = bf16[4,32,2048]{2,1,0:T(8,128)(2,1)S(1)} async-done(((bf16[4,32,2048]{2,1,0:T(8,128)(2,1)}), bf16[4,32,2048]{2,1,0:T(8,128)(2,1)S(1)}, u32[]{:S(2)}, u32[]{:S(2)}) %all-to-all-start.7) | async-done | bytes 524320 | tf_op jit(solution)/shard_map/all_to_all | solution.py:16
  20.2 0.7 broadcast_in_dim.16
  20.9 16.2 %all-to-all-start = ((bf16[4,32,384]{2,1,0:T(8,128)(2,1)}), bf16[4,32,384]{2,1,0:T(8,128)(2,1)S(1)}, u32[]{:S(2)}, u32[]{:S(2)}) async-start(bf16[4,32,384]{2,1,0:T(8,128)(2,1)} %broadcast_in_dim.16), calls=%async_computation | async-start | bytes 196608 | tf_op jit(solution)/shard_map/all_to_all | solution.py:16
  37.1 0.7 all-gather.2.cloned.1.call-update
  37.8 11.2 %all-to-all-done = bf16[4,32,384]{2,1,0:T(8,128)(2,1)S(1)} async-done(((bf16[4,32,384]{2,1,0:T(8,128)(2,1)}), bf16[4,32,384]{2,1,0:T(8,128)(2,1)S(1)}, u32[]{:S(2)}, u32[]{:S(2)}) %all-to-all-start) | async-done | bytes 98336 | tf_op jit(solution)/shard_map/all_to_all | solution.py:16
  49.0 10.6 %all_to_all.60 = bf16[4,4,32,384]{3,2,1,0:T(8,128)(2,1)S(1)} all-to-all(bf16[4,4,32,384]{3,2,1,0:T(8,128)(2,1)S(1)} %broadcast_in_dim.17), channel_id=1, replica_groups=mesh['zh'=4,'zl'=4,'y'=4,'x'=4,'c'=2] {'zl'}, dimensions={0} | all-to-all | bytes 786432 | tf_op jit(solution)/shard_map/all_to_all | solution.py:16
  59.6 1.4 broadcast_in_dim.18
  61.1 3.7 %all-to-all-start.2 = ((bf16[4,4,4,32,384]{4,3,1,2,0:T(8,128)(2,1)}), bf16[4,4,4,32,384]{4,3,1,2,0:T(8,128)(2,1)S(1)}, u32[]{:S(2)}, u32[]{:S(2)}) async-start(bf16[4,4,4,32,384]{4,3,1,2,0:T(8,128)(2,1)} %broadcast_in_dim.18), calls=%async_computation.2 | async-start | bytes 3145728 | tf_op jit(solution)/shard_map/all_to_all | solution.py:16
  64.8 0.3 fusion.7
  65.1 12.2 %all-to-all-done.2 = bf16[4,4,4,32,384]{4,3,1,2,0:T(8,128)(2,1)S(1)} async-done(((bf16[4,4,4,32,384]{4,3,1,2,0:T(8,128)(2,1)}), bf16[4,4,4,32,384]{4,3,1,2,0:T(8,128)(2,1)S(1)}, u32[]{:S(2)}, u32[]{:S(2)}) %all-to-all-start.2) | async-done | bytes 1572896 | tf_op jit(solution)/shard_map/all_to_all | solution.py:16
  77.3 0.2 copy.19
  77.6 1.8 fusion.41
  79.5 0.2 fusion.102
  79.7 0.2 fusion.32
  80.8 0.2 fusion.103
  81.0 0.2 fusion.40
  83.3 0.1 rev.2
  83.4 0.4 copy-done.2
  83.8 0.5 convolution_convert_fusion.1
  84.3 0.4 convolution_convert_fusion
  84.7 14.9 %all_to_all.61 = bf16[2,128,2048]{2,1,0:T(8,128)(2,1)S(1)} all-to-all(bf16[2,128,2048]{2,1,0:T(8,128)(2,1)S(1)} %bitcast.53), channel_id=1, replica_groups=mesh['zh'=4,'zl'=4,'y'=4,'x'=4,'c'=2] {'c'}, dimensions={0} | all-to-all | bytes 2097152 | tf_op jit(solution)/shard_map/all_to_all | solution.py:34
  99.7 1.1 reduce_sum.79
  100.8 4.0 %all-to-all-start.4 = ((bf16[4,32,2048]{2,1,0:T(8,128)(2,1)}), bf16[4,32,2048]{2,1,0:T(8,128)(2,1)S(1)}, u32[]{:S(2)}, u32[]{:S(2)}) async-start(bf16[4,32,2048]{2,1,0:T(8,128)(2,1)} %bitcast.17), calls=%async_computation.4 | async-start | bytes 1048576 | tf_op jit(solution)/shard_map/all_to_all | solution.py:37
  104.8 8.9 %all-to-all-done.4 = bf16[4,32,2048]{2,1,0:T(8,128)(2,1)S(1)} async-done(((bf16[4,32,2048]{2,1,0:T(8,128)(2,1)}), bf16[4,32,2048]{2,1,0:T(8,128)(2,1)S(1)}, u32[]{:S(2)}, u32[]{:S(2)}) %all-to-all-start.4) | async-done | bytes 524320 | tf_op jit(solution)/shard_map/all_to_all | solution.py:37
  113.7 0.1 convert_reduce_fusion.1
  113.8 0.1 multiply_reduce_fusion.1
  113.9 0.1 add_convert_fusion
  114.0 0.1 fusion.48
  114.2 0.1 fusion.50
  114.3 10.2 %all_to_all.62 = bf16[4,32,2048]{2,1,0:T(8,128)(2,1)S(1)} all-to-all(bf16[4,32,2048]{2,1,0:T(8,128)(2,1)S(1)} %broadcast_in_dim.19), channel_id=1, replica_groups=mesh['zh'=4,'zl'=4,'y'=4,'x'=4,'c'=2] {'x'}, dimensions={0} | all-to-all | bytes 1048576 | tf_op jit(solution)/shard_map/all_to_all | solution.py:16
  124.6 0.1 broadcast_in_dim.40
  124.7 6.8 %all_to_all.63 = bf16[2,4,32,2048]{3,2,1,0:T(8,128)(2,1)S(1)} all-to-all(bf16[2,4,32,2048]{3,2,1,0:T(8,128)(2,1)S(1)} %broadcast_in_dim.40), channel_id=1, replica_groups=mesh['zh'=4,'zl'=4,'y'=4,'x'=4,'c'=2] {'c'}, dimensions={0} | all-to-all | bytes 2097152 | tf_op jit(solution)/shard_map/all_to_all | solution.py:16
  131.5 16.2 %all-gather.2.cloned.1.call-done = bf16[2048,2048]{1,0:T(8,128)(2,1)} async-done(((bf16[128,2048]{1,0:T(8,128)(2,1)}), bf16[2048,2048]{1,0:T(8,128)(2,1)}) %all-gather.2.cloned.1.call-update) | async-done | bytes 8388624 | tf_op jit(solution)/shard_map/all_gather | solution.py:27
  147.7 5.8 %fusion.4 = bf16[256,2048]{1,0:T(8,128)(2,1)S(1)} fusion(bf16[2048,2048]{1,0:T(8,128)(2,1)} %all-gather.2.cloned.1.call-done, bf16[256,2048]{1,0:T(8,128)(2,1)S(1)} %bitcast.59), kind=kOutput, calls=%fused_computation.7 | convolution fusion | flops 2148794368 | bytes 10485760 | tf_op jit(solution)/shard_map/dot_general | solution.py:164
  153.5 5.0 %all_to_all.64 = bf16[2,128,2048]{2,1,0:T(8,128)(2,1)S(1)} all-to-all(bf16[2,128,2048]{2,1,0:T(8,128)(2,1)S(1)} %bitcast.60), channel_id=1, replica_groups=mesh['zh'=4,'zl'=4,'y'=4,'x'=4,'c'=2] {'c'}, dimensions={0} | all-to-all | bytes 2097152 | tf_op jit(solution)/shard_map/all_to_all | solution.py:34
  158.5 1.1 reduce_sum.83
  159.6 4.0 %all-to-all-start.9 = ((bf16[4,32,2048]{2,1,0:T(8,128)(2,1)}), bf16[4,32,2048]{2,1,0:T(8,128)(2,1)S(1)}, u32[]{:S(2)}, u32[]{:S(2)}) async-start(bf16[4,32,2048]{2,1,0:T(8,128)(2,1)} %bitcast.22), calls=%async_computation.9 | async-start | bytes 1048576 | tf_op jit(solution)/shard_map/all_to_all | solution.py:37
  163.5 8.9 %all-to-all-done.9 = bf16[4,32,2048]{2,1,0:T(8,128)(2,1)S(1)} async-done(((bf16[4,32,2048]{2,1,0:T(8,128)(2,1)}), bf16[4,32,2048]{2,1,0:T(8,128)(2,1)S(1)}, u32[]{:S(2)}, u32[]{:S(2)}) %all-to-all-start.9) | async-done | bytes 524320 | tf_op jit(solution)/shard_map/all_to_all | solution.py:37
  172.5 0.1 multiply_reduce_fusion
  172.7 0.1 fusion.51
  172.8 10.2 %all_to_all.65 = bf16[4,32,2048]{2,1,0:T(8,128)(2,1)S(1)} all-to-all(bf16[4,32,2048]{2,1,0:T(8,128)(2,1)S(1)} %broadcast_in_dim.42), channel_id=1, replica_groups=mesh['zh'=4,'zl'=4,'y'=4,'x'=4,'c'=2] {'x'}, dimensions={0} | all-to-all | bytes 1048576 | tf_op jit(solution)/shard_map/all_to_all | solution.py:16
  183.0 0.1 broadcast_in_dim.43
  183.2 6.8 %all_to_all.66 = bf16[2,4,32,2048]{3,2,1,0:T(8,128)(2,1)S(1)} all-to-all(bf16[2,4,32,2048]{3,2,1,0:T(8,128)(2,1)S(1)} %broadcast_in_dim.43), channel_id=1, replica_groups=mesh['zh'=4,'zl'=4,'y'=4,'x'=4,'c'=2] {'c'}, dimensions={0} | all-to-all | bytes 2097152 | tf_op jit(solution)/shard_map/all_to_all | solution.py:16
  190.0 1.0 copy.21
  (228 shorter events, 2.6 us)
Async XLA Ops:
  8.3 11.9 %all-to-all-start.7 = ((bf16[4,32,2048]{2,1,0:T(8,128)(2,1)}), bf16[4,32,2048]{2,1,0:T(8,128)(2,1)S(1)}, u32[]{:S(2)}, u32[]{:S(2)}) async-start(bf16[4,32,2048]{2,1,0:T(8,128)(2,1)} %broadcast_in_dim.41), calls=%async_computation.7 | async-start | bytes 1048576 | tf_op jit(solution)/shard_map/all_to_all | solution.py:16
  20.2 16.9 %copy-start = (bf16[4,32,2048]{2,1,0:T(8,128)(2,1)}, bf16[4,32,2048]{2,1,0:T(8,128)(2,1)S(1)}, u32[]{:S(2)}) copy-start(bf16[4,32,2048]{2,1,0:T(8,128)(2,1)S(1)} %all-to-all-done.7) | copy-start | bytes 1572868
  20.9 28.1 %all-to-all-start = ((bf16[4,32,384]{2,1,0:T(8,128)(2,1)}), bf16[4,32,384]{2,1,0:T(8,128)(2,1)S(1)}, u32[]{:S(2)}, u32[]{:S(2)}) async-start(bf16[4,32,384]{2,1,0:T(8,128)(2,1)} %broadcast_in_dim.16), calls=%async_computation | async-start | bytes 196608 | tf_op jit(solution)/shard_map/all_to_all | solution.py:16
  37.1 110.6 %all-gather.2.cloned.1.call-start = ((), (), s32[]{:S(2)}) async-start(), calls=%async_computation.12 | async-start | bytes 8912896 | tf_op jit(solution)/shard_map/all_gather | solution.py:27
  59.6 5.1 %copy-start.4 = (bf16[2048]{0:T(1024)(128)(2,1)S(1)}, bf16[2048]{0:T(1024)(128)(2,1)}, u32[]{:S(2)}) copy-start(bf16[2048]{0:T(1024)(128)(2,1)} %param.16) | copy-start | bytes 12292
  61.0 3.7 %copy-start.1 = (bf16[256,2048]{1,0:T(8,128)(2,1)S(1)}, bf16[256,2048]{1,0:T(8,128)(2,1)}, u32[]{:S(2)}) copy-start(bf16[256,2048]{1,0:T(8,128)(2,1)} %param.15) | copy-start | bytes 3145732
  61.0 4.0 %copy-start.9 = (f32[2,128]{1,0:T(2,128)S(1)}, f32[2,128]{1,0:T(2,128)}, u32[]{:S(2)}) copy-start(f32[2,128]{1,0:T(2,128)} %param.22) | copy-start | bytes 3076
  61.0 4.1 %copy-start.8 = (bf16[4,128]{1,0:T(4,128)(2,1)S(1)}, bf16[4,128]{1,0:T(4,128)(2,1)}, u32[]{:S(2)}) copy-start(bf16[4,128]{1,0:T(4,128)(2,1)} %param.19) | copy-start | bytes 3076
  61.1 16.3 %all-to-all-start.2 = ((bf16[4,4,4,32,384]{4,3,1,2,0:T(8,128)(2,1)}), bf16[4,4,4,32,384]{4,3,1,2,0:T(8,128)(2,1)S(1)}, u32[]{:S(2)}, u32[]{:S(2)}) async-start(bf16[4,4,4,32,384]{4,3,1,2,0:T(8,128)(2,1)} %broadcast_in_dim.18), calls=%async_computation.2 | async-start | bytes 3145728 | tf_op jit(solution)/shard_map/all_to_all | solution.py:16
  77.6 1.9 copy-start.10
  77.6 1.9 copy-start.11
  77.6 2.1 %copy-start.12 = (bf16[2,1,128,128]{3,2,1,0:T(8,128)(2,1)S(1)}, bf16[2,1,128,128]{3,2,1,0:T(8,128)(2,1)}, u32[]{:S(2)}) copy-start(bf16[2,1,128,128]{3,2,1,0:T(8,128)(2,1)} %param.21) | copy-start | bytes 196612
  79.9 1.3 copy-start.3
  81.3 1.4 slice-start
  82.5 1.2 copy-start.2
  84.7 20.0 %copy-start.5 = (bf16[2048]{0:T(1024)(128)(2,1)S(1)}, bf16[2048]{0:T(1024)(128)(2,1)}, u32[]{:S(2)}) copy-start(bf16[2048]{0:T(1024)(128)(2,1)} %param.25) | copy-start | bytes 12292
  84.7 20.0 %copy-start.6 = (bf16[2048]{0:T(1024)(128)(2,1)S(1)}, bf16[2048]{0:T(1024)(128)(2,1)}, u32[]{:S(2)}) copy-start(bf16[2048]{0:T(1024)(128)(2,1)} %param.26) | copy-start | bytes 12292
  100.8 12.9 %all-to-all-start.4 = ((bf16[4,32,2048]{2,1,0:T(8,128)(2,1)}), bf16[4,32,2048]{2,1,0:T(8,128)(2,1)S(1)}, u32[]{:S(2)}, u32[]{:S(2)}) async-start(bf16[4,32,2048]{2,1,0:T(8,128)(2,1)} %bitcast.17), calls=%async_computation.4 | async-start | bytes 1048576 | tf_op jit(solution)/shard_map/all_to_all | solution.py:37
  153.5 10.1 %copy-start.7 = (bf16[2048]{0:T(1024)(128)(2,1)S(1)}, bf16[2048]{0:T(1024)(128)(2,1)}, u32[]{:S(2)}) copy-start(bf16[2048]{0:T(1024)(128)(2,1)} %param.29) | copy-start | bytes 12292
  159.6 12.9 %all-to-all-start.9 = ((bf16[4,32,2048]{2,1,0:T(8,128)(2,1)}), bf16[4,32,2048]{2,1,0:T(8,128)(2,1)S(1)}, u32[]{:S(2)}, u32[]{:S(2)}) async-start(bf16[4,32,2048]{2,1,0:T(8,128)(2,1)} %bitcast.22), calls=%async_computation.9 | async-start | bytes 1048576 | tf_op jit(solution)/shard_map/all_to_all | solution.py:37
Sparse Core Ops, SparseCore 0:
  40.0 107.6 all-gather.1
where the time goes:
time: 199 us; the launch traced here: 198 us
  blocking collectives  64.5 us (32%)
  waiting for transfers between devices  64.2 us (32%)
  starting transfers between devices  32.8 us (16%)
  between operations  14.6 us (7%)
  matrix products  9.29 us (5%)
  local copies, waits for them, and re-layouts  6.69 us (3%)
  other arithmetic  5.67 us (3%)
    all_to_all x5, blocking collectives, spread(): return lax.all_to_all(copies, axis, split_axis=0, concat_axis=0, tiled=True)  44.6 us
    all_to_all x3, waiting for transfers between devices, spread(): return lax.all_to_all(copies, axis, split_axis=0, concat_axis=0, tiled=True)  29.5 us
    all_to_all x3, starting transfers between devices, spread(): return lax.all_to_all(copies, axis, split_axis=0, concat_axis=0, tiled=True)  24.9 us
    all_to_all x2, blocking collectives, summed_rows(): pair = lax.all_to_all(halves, 'c', split_axis=0, concat_axis=0, tiled=True)  19.9 us
    all_to_all x2, waiting for transfers between devices, summed_rows(): lax.all_to_all(quarters, 'x', split_axis=0, concat_axis=0, tiled=True)  17.8 us
    all_gather x1, waiting for transfers between devices, feedforward_weights(): return lax.all_gather(near, Z, axis=0, tiled=True)  16.2 us
    all_to_all x2, starting transfers between devices, summed_rows(): lax.all_to_all(quarters, 'x', split_axis=0, concat_axis=0, tiled=True)  7.93 us
    dot_general x1, matrix products, per_device(): lax.dot_general(lifted, forward[:, hidden_units:], across, preferred_elem...  5.81 us
  transfers between devices with their start and end apart: 6, of which 6 were waited for; matrix products, arithmetic and copies ran while one was open for 5% of the time, Pallas kernels for 0%

commit v1 on v0

--- a/solution.py
+++ b/solution.py
@@ -24,7 +24,7 @@
 
 def feedforward_weights(array):
     near = spread(array, "y").reshape(-1, array.shape[-1])
-    return lax.all_gather(near, Z, axis=0, tiled=True)
+    return jnp.concatenate(lax.all_to_all(jnp.stack([near] * lax.axis_size(Z)), Z, 0, 0), axis=0)
 
 
 def summed_rows(partial):

time: 199 us -> 566 us (2.84)
  blocking collectives: 64.5 us -> 462 us
  waiting for transfers between devices: 64.2 us -> 40.4 us
  starting transfers between devices: 32.8 us -> 15.3 us
  between operations: 14.6 us -> 1.01 us
  local copies, waits for them, and re-layouts: 6.69 us -> 18.1 us
  other arithmetic: 5.67 us -> 13.4 us
    all_to_all x0 -> x1, blocking collectives: none -> 366 us  [feedforward_weights(): lax.all_to_all(jnp.stack([near] * lax.axis_size(Z)), Z, 0, 0)]
    all_to_all x5 -> x6, blocking collectives: 44.6 us -> 73.7 us  [spread(): return lax.all_to_all(copies, axis, split_axis=0, concat_axis=0, tiled=True)]
    all_to_all x3 -> x2, starting transfers between devices: 24.9 us -> 7.79 us  [spread(): return lax.all_to_all(copies, axis, split_axis=0, concat_axis=0, tiled=True)]
    all_gather x1 -> x0, waiting for transfers between devices: 16.2 us -> none  [feedforward_weights(): return lax.all_gather(near, Z, axis=0, tiled=True)]
    slice x99 -> x98, local copies, waits for them, and re-layouts: 1.37 us -> 12.5 us  [linear_recurrence(): lax.associative_scan(combine, (decay, drive), reverse=reversed_scan, axis=0)]
    all_to_all x3 -> x2, waiting for transfers between devices: 29.5 us -> 22.4 us  [spread(): return lax.all_to_all(copies, axis, split_axis=0, concat_axis=0, tiled=True)]
  transfers between devices with their start and end apart: 6 -> 4, of which waited for: 6 -> 4; matrix products, arithmetic and copies ran while one was open for 5% -> 0% of each run, Pallas kernels for 0% -> 0%
where the time goes in v1:
time: 566 us; the launch traced here: 565 us
  blocking collectives  462 us (82%)
  waiting for transfers between devices  40.4 us (7%)
  local copies, waits for them, and re-layouts  18.1 us (3%)
  starting transfers between devices  15.3 us (3%)
  matrix products  14.3 us (3%)
  other arithmetic  13.4 us (2%)
    all_to_all x1, blocking collectives, feedforward_weights(): lax.all_to_all(jnp.stack([near] * lax.axis_size(Z)), Z, 0, 0)  366 us
    all_to_all x6, blocking collectives, spread(): return lax.all_to_all(copies, axis, split_axis=0, concat_axis=0, tiled=True)  73.7 us
    all_to_all x2, blocking collectives, summed_rows(): pair = lax.all_to_all(halves, 'c', split_axis=0, concat_axis=0, tiled=True)  22.6 us
    all_to_all x2, waiting for transfers between devices, spread(): return lax.all_to_all(copies, axis, split_axis=0, concat_axis=0, tiled=True)  22.4 us
    all_to_all x2, waiting for transfers between devices, summed_rows(): lax.all_to_all(quarters, 'x', split_axis=0, concat_axis=0, tiled=True)  18 us
    slice x98, local copies, waits for them, and re-layouts, linear_recurrence(): lax.associative_scan(combine, (decay, drive), reverse=reversed_scan, axis=0)  12.5 us
  transfers between devices with their start and end apart: 4, of which 4 were waited for; matrix products, arithmetic and copies ran while one was open for 0% of the time, Pallas kernels for 0%

profile of v1, /device:TPU:1, one launch (start us, length us, event | category | flops | bytes accessed | tf_op | source)
XLA Modules:
  0.0 564.7 jit_solution(11586163537278222041)
XLA Ops:
  0.0 0.7 pad_maximum_fusion.5
  0.7 28.0 %all_to_all.65 = bf16[4,32,384]{2,1,0:T(8,128)(2,1)S(1)} all-to-all(bf16[4,32,384]{2,1,0:T(8,128)(2,1)S(1)} %broadcast_in_dim.16), channel_id=1, replica_groups=mesh['zh'=4,'zl'=4,'y'=4,'x'=4,'c'=2] {'zh'}, dimensions={0} | all-to-all | bytes 196608 | tf_op jit(solution)/shard_map/all_to_all | solution.py:16
  28.8 11.3 %all_to_all.66 = bf16[4,4,32,384]{3,2,1,0:T(8,128)(2,1)S(1)} all-to-all(bf16[4,4,32,384]{3,2,1,0:T(8,128)(2,1)S(1)} %broadcast_in_dim.17), channel_id=1, replica_groups=mesh['zh'=4,'zl'=4,'y'=4,'x'=4,'c'=2] {'zl'}, dimensions={0} | all-to-all | bytes 786432 | tf_op jit(solution)/shard_map/all_to_all | solution.py:16
  40.2 1.4 broadcast_in_dim.18
  41.5 4.3 all-to-all-start.2
  46.8 15.3 %all-to-all-done.2 = bf16[4,4,4,32,384]{4,3,1,2,0:T(8,128)(2,1)S(1)} async-done(((bf16[4,4,4,32,384]{4,3,1,2,0:T(8,128)(2,1)}), bf16[4,4,4,32,384]{4,3,1,2,0:T(8,128)(2,1)S(1)}, u32[]{:S(2)}, u32[]{:S(2)}) %all-to-all-start.2) | async-done | bytes 1572896 | tf_op jit(solution)/shard_map/all_to_all | solution.py:16
  62.3 1.8 convolution_convert_fusion.1
  65.1 0.9 fusion.103
  66.0 1.1 fusion.40
  67.4 0.6 slice.580
  68.1 0.6 slice.551
  70.6 0.6 slice.568
  71.8 0.6 slice.566
  74.1 0.6 slice.578
  74.7 0.6 slice.545
  77.4 1.8 fusion.102
  79.3 1.1 fusion.32
  81.1 0.7 fusion.101
  81.8 0.8 fusion.98
  84.5 0.7 multiply_add_fusion.12
  85.1 0.6 pad_maximum_fusion.13
  85.8 0.7 multiply_add_fusion.8
  86.5 0.7 pad_maximum_fusion.11
  87.2 0.7 fusion.79
  87.9 0.6 pad_maximum_fusion.9
  88.5 0.7 fusion.77
  89.3 0.7 pad_maximum_fusion.7
  90.0 0.6 pad_maximum_fusion.4
  90.7 0.6 pad_maximum_fusion.2
  92.5 9.8 %all_to_all.67 = bf16[2,128,2048]{2,1,0:T(8,128)(2,1)S(1)} all-to-all(bf16[2,128,2048]{2,1,0:T(8,128)(2,1)S(1)} %bitcast.55), channel_id=1, replica_groups=mesh['zh'=4,'zl'=4,'y'=4,'x'=4,'c'=2] {'c'}, dimensions={0} | all-to-all | bytes 2097152 | tf_op jit(solution)/shard_map/all_to_all | solution.py:34
  102.3 1.1 reduce_sum.79
  103.4 4.0 all-to-all-start.4
  107.5 8.9 %all-to-all-done.4 = bf16[4,32,2048]{2,1,0:T(8,128)(2,1)S(1)} async-done(((bf16[4,32,2048]{2,1,0:T(8,128)(2,1)}), bf16[4,32,2048]{2,1,0:T(8,128)(2,1)S(1)}, u32[]{:S(2)}, u32[]{:S(2)}) %all-to-all-start.4) | async-done | bytes 524320 | tf_op jit(solution)/shard_map/all_to_all | solution.py:37
  116.3 0.8 broadcast_in_dim.41
  117.2 3.5 all-to-all-start.7
  121.3 7.1 %all-to-all-done.7 = bf16[4,32,2048]{2,1,0:T(8,128)(2,1)S(1)} async-done(((bf16[4,32,2048]{2,1,0:T(8,128)(2,1)}), bf16[4,32,2048]{2,1,0:T(8,128)(2,1)S(1)}, u32[]{:S(2)}, u32[]{:S(2)}) %all-to-all-start.7) | async-done | bytes 524320 | tf_op jit(solution)/shard_map/all_to_all | solution.py:16
  128.4 9.3 %all_to_all.68 = bf16[4,32,2048]{2,1,0:T(8,128)(2,1)S(1)} all-to-all(bf16[4,32,2048]{2,1,0:T(8,128)(2,1)S(1)} %broadcast_in_dim.19), channel_id=1, replica_groups=mesh['zh'=4,'zl'=4,'y'=4,'x'=4,'c'=2] {'x'}, dimensions={0} | all-to-all | bytes 1048576 | tf_op jit(solution)/shard_map/all_to_all | solution.py:16
  137.9 8.0 %all_to_all.69 = bf16[2,4,32,2048]{3,2,1,0:T(8,128)(2,1)S(1)} all-to-all(bf16[2,4,32,2048]{3,2,1,0:T(8,128)(2,1)S(1)} %broadcast_in_dim.40), channel_id=1, replica_groups=mesh['zh'=4,'zl'=4,'y'=4,'x'=4,'c'=2] {'c'}, dimensions={0} | all-to-all | bytes 2097152 | tf_op jit(solution)/shard_map/all_to_all | solution.py:16
  145.9 1.0 stack.3
  147.0 365.9 %all_to_all.70 = bf16[16,128,2048]{2,1,0:T(8,128)(2,1)} all-to-all(bf16[16,128,2048]{2,1,0:T(8,128)(2,1)S(1)} %stack.3), channel_id=1, replica_groups=mesh['zh'=4,'zl'=4,'y'=4,'x'=4,'c'=2] {'zh','zl'}, dimensions={0} | all-to-all | bytes 16777216 | tf_op jit(solution)/shard_map/all_to_all | solution.py:27
  512.9 6.8 %fusion.4 = bf16[256,2048]{1,0:T(8,128)(2,1)} fusion(bf16[2048,2048]{1,0:T(8,128)(2,1)} %bitcast.54, bf16[256,2048]{1,0:T(8,128)(2,1)S(1)} %bitcast.61), kind=kOutput, calls=%fused_computation.7 | convolution fusion | flops 2148794368 | bytes 10485760 | tf_op jit(solution)/shard_map/dot_general | solution.py:164
  519.7 12.7 %all_to_all.71 = bf16[2,128,2048]{2,1,0:T(8,128)(2,1)S(1)} all-to-all(bf16[2,128,2048]{2,1,0:T(8,128)(2,1)} %bitcast.62), channel_id=1, replica_groups=mesh['zh'=4,'zl'=4,'y'=4,'x'=4,'c'=2] {'c'}, dimensions={0} | all-to-all | bytes 2097152 | tf_op jit(solution)/shard_map/all_to_all | solution.py:34
  532.4 1.1 reduce_sum.83
  533.5 3.5 all-to-all-start.10
  537.0 9.1 %all-to-all-done.10 = bf16[4,32,2048]{2,1,0:T(8,128)(2,1)S(1)} async-done(((bf16[4,32,2048]{2,1,0:T(8,128)(2,1)}), bf16[4,32,2048]{2,1,0:T(8,128)(2,1)S(1)}, u32[]{:S(2)}, u32[]{:S(2)}) %all-to-all-start.10) | async-done | bytes 524320 | tf_op jit(solution)/shard_map/all_to_all | solution.py:37
  546.5 10.7 %all_to_all.72 = bf16[4,32,2048]{2,1,0:T(8,128)(2,1)S(1)} all-to-all(bf16[4,32,2048]{2,1,0:T(8,128)(2,1)S(1)} %broadcast_in_dim.42), channel_id=1, replica_groups=mesh['zh'=4,'zl'=4,'y'=4,'x'=4,'c'=2] {'x'}, dimensions={0} | all-to-all | bytes 1048576 | tf_op jit(solution)/shard_map/all_to_all | solution.py:16
  557.4 6.3 %all_to_all.73 = bf16[2,4,32,2048]{3,2,1,0:T(8,128)(2,1)S(1)} all-to-all(bf16[2,4,32,2048]{3,2,1,0:T(8,128)(2,1)S(1)} %broadcast_in_dim.43), channel_id=1, replica_groups=mesh['zh'=4,'zl'=4,'y'=4,'x'=4,'c'=2] {'c'}, dimensions={0} | all-to-all | bytes 2097152 | tf_op jit(solution)/shard_map/all_to_all | solution.py:16
  563.7 1.0 copy.21
  (235 shorter events, 13.5 us)
Async XLA Ops:
  40.2 5.7 %copy-start.6 = (bf16[2048]{0:T(1024)(128)(2,1)S(1)}, bf16[2048]{0:T(1024)(128)(2,1)}, u32[]{:S(2)}) copy-start(bf16[2048]{0:T(1024)(128)(2,1)} %param.16) | copy-start | bytes 12292
  41.5 4.3 copy-start
  41.5 4.6 copy-start.11
  41.5 5.2 copy-start.10
  41.5 20.5 %all-to-all-start.2 = ((bf16[4,4,4,32,384]{4,3,1,2,0:T(8,128)(2,1)}), bf16[4,4,4,32,384]{4,3,1,2,0:T(8,128)(2,1)S(1)}, u32[]{:S(2)}, u32[]{:S(2)}) async-start(bf16[4,4,4,32,384]{4,3,1,2,0:T(8,128)(2,1)} %broadcast_in_dim.18), calls=%async_computation.2 | async-start | bytes 3145728 | tf_op jit(solution)/shard_map/all_to_all | solution.py:16
  62.3 1.8 copy-start.1
  64.1 1.0 copy-start.15
  64.1 0.9 copy-start.16
  64.2 1.8 copy-start.17
  70.6 9.8 %copy-start.4 = (f32[4,128]{1,0:T(4,128)}, f32[4,128]{1,0:T(4,128)S(1)}, u32[]{:S(2)}) copy-start(f32[4,128]{1,0:T(4,128)S(1)} %get-tuple-element.32) | copy-start | bytes 6148
  70.6 9.8 %copy-start.5 = (f32[4,128]{1,0:T(4,128)}, f32[4,128]{1,0:T(4,128)S(1)}, u32[]{:S(2)}) copy-start(f32[4,128]{1,0:T(4,128)S(1)} %get-tuple-element.31) | copy-start | bytes 6148
  84.4 7.2 %copy-start.13 = (f32[1,128]{1,0:T(1,128)S(1)}, f32[1,128]{1,0:T(1,128)}, u32[]{:S(2)}) copy-start(f32[1,128]{1,0:T(1,128)} %slice.595) | copy-start | bytes 1540
  84.4 7.3 %copy-start.12 = (f32[1,128]{1,0:T(1,128)S(1)}, f32[1,128]{1,0:T(1,128)}, u32[]{:S(2)}) copy-start(f32[1,128]{1,0:T(1,128)} %slice.594) | copy-start | bytes 1540
  89.3 2.3 copy-start.14
  92.4 15.0 %copy-start.7 = (bf16[2048]{0:T(1024)(128)(2,1)S(1)}, bf16[2048]{0:T(1024)(128)(2,1)}, u32[]{:S(2)}) copy-start(bf16[2048]{0:T(1024)(128)(2,1)} %param.25) | copy-start | bytes 12292
  92.4 15.0 %copy-start.8 = (bf16[2048]{0:T(1024)(128)(2,1)S(1)}, bf16[2048]{0:T(1024)(128)(2,1)}, u32[]{:S(2)}) copy-start(bf16[2048]{0:T(1024)(128)(2,1)} %param.26) | copy-start | bytes 12292
  92.4 15.0 %copy-start.2 = (bf16[1024,32]{0,1:T(8,128)(2,1)S(1)}, bf16[1024,32]{0,1:T(8,128)(2,1)}, u32[]{:S(2)}) copy-start(bf16[1024,32]{0,1:T(8,128)(2,1)} %param.28) | copy-start | bytes 196612
  92.5 15.0 %copy-start.3 = (bf16[32,1024]{1,0:T(8,128)(2,1)S(1)}, bf16[32,1024]{1,0:T(8,128)(2,1)}, u32[]{:S(2)}) copy-start(bf16[32,1024]{1,0:T(8,128)(2,1)} %param.27) | copy-start | bytes 196612
  103.4 12.9 %all-to-all-start.4 = ((bf16[4,32,2048]{2,1,0:T(8,128)(2,1)}), bf16[4,32,2048]{2,1,0:T(8,128)(2,1)S(1)}, u32[]{:S(2)}, u32[]{:S(2)}) async-start(bf16[4,32,2048]{2,1,0:T(8,128)(2,1)} %bitcast.17), calls=%async_computation.4 | async-start | bytes 1048576 | tf_op jit(solution)/shard_map/all_to_all | solution.py:37
  117.2 11.2 %all-to-all-start.7 = ((bf16[4,32,2048]{2,1,0:T(8,128)(2,1)}), bf16[4,32,2048]{2,1,0:T(8,128)(2,1)S(1)}, u32[]{:S(2)}, u32[]{:S(2)}) async-start(bf16[4,32,2048]{2,1,0:T(8,128)(2,1)} %broadcast_in_dim.41), calls=%async_computation.7 | async-start | bytes 1048576 | tf_op jit(solution)/shard_map/all_to_all | solution.py:16
  519.7 17.3 %copy-start.9 = (bf16[2048]{0:T(1024)(128)(2,1)S(1)}, bf16[2048]{0:T(1024)(128)(2,1)}, u32[]{:S(2)}) copy-start(bf16[2048]{0:T(1024)(128)(2,1)} %param.29) | copy-start | bytes 12292
  533.5 12.6 %all-to-all-start.10 = ((bf16[4,32,2048]{2,1,0:T(8,128)(2,1)}), bf16[4,32,2048]{2,1,0:T(8,128)(2,1)S(1)}, u32[]{:S(2)}, u32[]{:S(2)}) async-start(bf16[4,32,2048]{2,1,0:T(8,128)(2,1)} %bitcast.23), calls=%async_computation.10 | async-start | bytes 1048576 | tf_op jit(solution)/shard_map/all_to_all | solution.py:37
